TPU v7x, 32 devices: a whole 2x2x4 slice. The times are simulated.
32 devices in a mesh: sp: 8 (over z, x), dp: 4 (over y, core).
Axes of the slice: x: 2, y: 2, z: 4, core: 2. Of those that a mesh axis runs over, the one named last changes fastest.
Arguments:
- queries: bfloat16 [4, 1024, 2048], P('dp', 'sp'), may hold values from -6 to 6
- keys: bfloat16 [4, 1024, 2048], P('dp', 'sp'), may hold values from -6 to 6
- values: bfloat16 [4, 1024, 2048], P('dp', 'sp'), may hold values from -6 to 6
- gate_totals: float32 [4, 1024, 32], P('dp', 'sp'), may hold values from -1024 to 0, as said below
- w_out: bfloat16 [2048, 2048], P(None, 'dp'), may hold values from -1 to 1
Outputs:
- mixed: bfloat16 [4, 1024, 2048], P('dp', 'sp')
Inputs may be any that keep to these rules, and one draw needn't show every extreme that they name: `gate_totals`: never rising along a sequence.
All inputs are finite; a program needn't handle non-finite values.
Results may differ from a plain program's by a relative error of at most 0.0053.
Values may be sent and summed in bfloat16 or wider, within the bound.
A program may use at most 64 MiB of HBM per device.

v0:
```python
import jax
import jax.numpy as jnp
from jax import lax
from jax.sharding import PartitionSpec as P

HEAD_DIM = 64


def attend(queries, key_rows, value_rows, totals):
    length = queries.shape[0]
    block_rows = min(length, 512)
    pieces = []
    for begin_row in range(0, length, block_rows):
        end_row = begin_row + block_rows
        scaled = queries[begin_row:end_row] * jnp.bfloat16(HEAD_DIM ** (-0.5))
        scores = jnp.einsum(
            "qhd,khd->hqk", scaled, key_rows[:end_row], preferred_element_type=jnp.float32
        )
        causal = jnp.arange(end_row)[None, :] <= (begin_row + jnp.arange(block_rows))[:, None]
        scores = jnp.where(
            causal[None],
            scores
            + jnp.transpose(totals[begin_row:end_row])[:, :, None]
            - jnp.transpose(totals[:end_row])[:, None, :],
            -jnp.inf,
        )
        biggest = jnp.max(scores, axis=-1, keepdims=True)
        expo = jnp.exp(scores - biggest)
        summed = jnp.sum(expo, axis=-1)
        weights = expo.astype(jnp.bfloat16)
        output = jnp.einsum(
            "hqk,khd->qhd", weights, value_rows[:end_row], preferred_element_type=jnp.float32
        )
        output = output / jnp.transpose(summed)[:, :, None]
        pieces.append(output.astype(jnp.bfloat16))
    return jnp.concatenate(pieces, axis=0).reshape(length, -1)


def local(queries, keys, values, gate_totals, w_out):
    moved = (
        lax.all_to_all(queries, "sp", split_axis=2, concat_axis=1, tiled=True),
        lax.all_to_all(keys, "sp", split_axis=2, concat_axis=1, tiled=True),
        lax.all_to_all(values, "sp", split_axis=2, concat_axis=1, tiled=True),
    )
    totals = lax.all_to_all(gate_totals, "sp", split_axis=2, concat_axis=1, tiled=True)
    held, length = (moved[0].shape[0], moved[0].shape[1])
    query_heads, key_heads, value_heads = [
        part_array[0].reshape(length, -1, HEAD_DIM) for part_array in moved
    ]
    outputs = [attend(query_heads, key_heads, value_heads, totals[0])]
    attended = jnp.stack(outputs, axis=0)
    local_rows = lax.all_to_all(attended, "sp", split_axis=1, concat_axis=2, tiled=True)
    flat_rows = local_rows.reshape(-1, local_rows.shape[2])
    mixed = jnp.dot(
        flat_rows,
        lax.all_gather(w_out, "dp", axis=1, tiled=True),
        preferred_element_type=jnp.float32,
    )
    return mixed.astype(jnp.bfloat16).reshape(local_rows.shape[0], local_rows.shape[1], -1)


def solution(mesh):
    placed = (
        P("dp", "sp", None),
        P("dp", "sp", None),
        P("dp", "sp", None),
        P("dp", "sp", None),
        P(None, "dp"),
    )
    return jax.shard_map(
        local, mesh=mesh, in_specs=placed, out_specs=P("dp", "sp", None), check_vma=False
    )
```

profile of v0, /device:TPU:0, one launch (start us, length us, event | category | flops | bytes accessed | tf_op | source)
XLA Modules:
  0.0 138.5 jit_solution(7458643636415226542)
XLA Ops:
  7.3 7.3 %all-to-all-start.2 = ((f32[1,128,32]{1,0,2:T(1,128)}), f32[1,128,32]{1,0,2:T(1,128)S(1)}, u32[]{:S(2)}, u32[]{:S(2)}) async-start(f32[1,128,32]{1,0,2:T(1,128)} %bitcast.98), calls=%async_computation.2 | async-start | bytes 32768 | tf_op jit(solution)/shard_map/all_to_all | solution.py:45
  14.6 2.3 %copy.32 = bf16[1,128,2048]{1,0,2:T(2,128)(2,1)S(1)} copy(bf16[1,128,2048]{2,1,0:T(8,128)(2,1)} %param.6) | data formatting | bytes 1048576 | tf_op args[1]
  17.5 11.6 %reduce.2 = bf16[2048,128]{1,0:T(8,128)(2,1)S(1)} reduce(bf16[2048,1,128]{2,1,0:T(2,128)(2,1)S(1)} %bitcast.83, bf16[]{:T(256)} %broadcast.36), dimensions={1}, to_apply=%bitcast.66.reduce_sub_computation | reduce | bytes 1048578
  29.0 1.0 reshape.70
  30.0 6.0 %all-to-all-start.1 = ((bf16[8,2,16384]{2,1,0:T(2,128)(2,1)}), bf16[8,2,16384]{2,1,0:T(2,128)(2,1)S(1)}, u32[]{:S(2)}, u32[]{:S(2)}) async-start(bf16[8,2,16384]{2,1,0:T(2,128)(2,1)} %reshape.70), calls=%async_computation.1 | async-start | bytes 1048576 | tf_op jit(solution)/shard_map/all_to_all | solution.py:42
  36.8 11.5 %reduce = bf16[2048,128]{1,0:T(8,128)(2,1)S(1)} reduce(bf16[2048,1,128]{2,1,0:T(2,128)(2,1)S(1)} %bitcast.85, bf16[]{:T(256)} %broadcast.36), dimensions={1}, to_apply=%bitcast.62.reduce_sub_computation | reduce | bytes 1048578
  48.3 0.9 reshape.66
  50.0 5.2 %all-to-all-start.3 = ((bf16[8,2,16384]{2,1,0:T(2,128)(2,1)}), bf16[8,2,16384]{2,1,0:T(2,128)(2,1)S(1)}, u32[]{:S(2)}, u32[]{:S(2)}) async-start(bf16[8,2,16384]{2,1,0:T(2,128)(2,1)} %reshape.66), calls=%async_computation.3 | async-start | bytes 1048576 | tf_op jit(solution)/shard_map/all_to_all | solution.py:43
  56.0 11.5 %reduce.1 = bf16[2048,128]{1,0:T(8,128)(2,1)S(1)} reduce(bf16[2048,1,128]{2,1,0:T(2,128)(2,1)S(1)} %bitcast.86, bf16[]{:T(256)} %broadcast.36), dimensions={1}, to_apply=%bitcast.64.reduce_sub_computation | reduce | bytes 1048578
  67.5 1.0 reshape.68
  68.6 5.9 %all-to-all-start = ((bf16[8,2,16384]{2,1,0:T(2,128)(2,1)}), bf16[8,2,16384]{2,1,0:T(2,128)(2,1)S(1)}, u32[]{:S(2)}, u32[]{:S(2)}) async-start(bf16[8,2,16384]{2,1,0:T(2,128)(2,1)} %reshape.68), calls=%async_computation | async-start | bytes 1048576 | tf_op jit(solution)/shard_map/all_to_all | solution.py:41
  78.3 8.9 %all-to-all-done = bf16[8,2,16384]{2,1,0:T(2,128)(2,1)S(1)} async-done(((bf16[8,2,16384]{2,1,0:T(2,128)(2,1)}), bf16[8,2,16384]{2,1,0:T(2,128)(2,1)S(1)}, u32[]{:S(2)}, u32[]{:S(2)}) %all-to-all-start) | async-done | bytes 524320 | tf_op jit(solution)/shard_map/all_to_all | solution.py:41
  88.1 0.8 mul.15
  89.0 1.0 reshape_squeeze.7
  91.2 1.2 fusion.8
  92.3 1.2 fusion.6
  93.6 1.4 %fusion.22 = bf16[512,4,64]{0,2,1:T(8,128)(2,1)S(1)} fusion(bf16[512,4,64]{0,2,1:T(8,128)(2,1)S(1)} %slice.39, f32[4,512,512]{1,2,0:T(8,128)S(1)} %get-tuple-element.12, f32[4,512]{1,0:T(4,128)S(1)} %get-tuple-element.11, f32[4,512]{1,0:T(4,128)S(1)} %get-tuple-element.7, pred[512,512]{0,1:T(8,128)(4,1)S(1)} %iota_compare_fusion.1, f32[512,4]{0,1:T(4,128)S(1)} %bitcast.100), kind=kOutput, calls=%fused_computation.21 | convolution fusion | flops 139722752 | bytes 5005312 | tf_op jit(solution)/shard_map/hqk,khd->qhd/dot_general | solution.py:31
  95.1 2.2 %fusion.2 = (f32[4,512]{1,0:T(4,128)S(1)}, f32[4,512,1024]{2,1,0:T(8,128)S(1)}) fusion(f32[4,1024]{1,0:T(4,128)S(1)} %bitcast.95, f32[4,512]{1,0:T(4,128)S(1)} %get-tuple-element.8, pred[512,1024]{1,0:T(8,128)(4,1)S(1)} %iota_compare_fusion, bf16[512,4,64]{0,2,1:T(8,128)(2,1)S(1)} %copy-done.5, bf16[1024,4,64]{0,2,1:T(8,128)(2,1)S(1)} %copy-done.4), kind=kOutput, calls=%fused_computation.4 | convolution fusion | flops 276822016 | bytes 9732096 | tf_op jit(solution)/shard_map/qhd,khd->hqk/dot_general | solution.py:16
  97.3 2.8 %fusion = f32[4,512]{1,0:T(4,128)S(1)} fusion(f32[4,512,1024]{2,1,0:T(8,128)S(1)} %get-tuple-element.10, f32[4,512]{1,0:T(4,128)S(1)} %get-tuple-element.9, f32[4,1024]{1,0:T(4,128)S(1)} %bitcast.96, f32[4,512]{1,0:T(4,128)S(1)} %get-tuple-element.8, pred[512,1024]{1,0:T(8,128)(4,1)S(1)} %iota_compare_fusion), kind=kLoop, calls=%fused_computation.2 | loop fusion | flops 10483712 | bytes 8953856 | tf_op jit(solution)/shard_map/reduce_sum | solution.py:29
  100.1 2.8 %fusion.28 = bf16[512,4,64]{0,2,1:T(8,128)(2,1)S(1)} fusion(bf16[1024,4,64]{0,2,1:T(8,128)(2,1)S(1)} %reshape_squeeze.8, f32[4,512,1024]{2,1,0:T(8,128)S(1)} %get-tuple-element.10, f32[4,512]{1,0:T(4,128)S(1)} %get-tuple-element.9, f32[4,1024]{1,0:T(4,128)S(1)} %bitcast.97, f32[4,512]{1,0:T(4,128)S(1)} %get-tuple-element.8, ...), kind=kOutput, calls=%fused_computation.23 | convolution fusion | flops 279183360 | bytes 9740288 | tf_op jit(solution)/shard_map/hqk,khd->qhd/dot_general | solution.py:31
  103.0 1.1 copy.41
  104.1 3.8 %reduce.3 = bf16[1024,256]{1,0:T(8,128)(2,1)S(1)} reduce(bf16[1024,1,256]{2,1,0:T(2,128)(2,1)S(1)} %bitcast.84, bf16[]{:T(256)} %broadcast.36), dimensions={1}, to_apply=%bitcast.68.reduce_sub_computation | reduce | bytes 1048578
  108.0 17.2 %all_to_all.75 = bf16[8,2,16384]{2,1,0:T(2,128)(2,1)S(1)} all-to-all(bf16[8,2,16384]{2,1,0:T(2,128)(2,1)S(1)} %reshape.72), channel_id=1, replica_groups=mesh['sp'=8,'dp'=4] {'sp'}, dimensions={0} | all-to-all | bytes 1048576 | tf_op jit(solution)/shard_map/all_to_all | solution.py:52
  126.2 5.5 %fusion.9 = bf16[1,128,2048]{2,1,0:T(8,128)(2,1)} fusion(bf16[128,2048]{0,1:T(8,128)(2,1)S(1)} %bitcast.78, bf16[2048,2048]{1,0:T(8,128)(2,1)} %all-gather.2.cloned.1.call-done), kind=kOutput, calls=%fused_computation.13 | convolution fusion | flops 1074003968 | bytes 9437184 | tf_op jit(solution)/shard_map/dot_general | solution.py:54
  (49 shorter events, 10.6 us)
Async XLA Ops:
  6.5 29.5 %copy-start.2 = (bf16[1,128,2048]{2,1,0:T(8,128)(2,1)S(1)}, bf16[1,128,2048]{2,1,0:T(8,128)(2,1)}, u32[]{:S(2)}) copy-start(bf16[1,128,2048]{2,1,0:T(8,128)(2,1)} %param.7) | copy-start | bytes 1572868
  6.5 119.6 %all-gather.2.cloned.1.call-start = ((), (), s32[]{:S(2)}) async-start(), calls=%async_computation.5 | async-start | bytes 10485760 | tf_op jit(solution)/shard_map/all_gather | solution.py:56
  7.3 22.8 %all-to-all-start.2 = ((f32[1,128,32]{1,0,2:T(1,128)}), f32[1,128,32]{1,0,2:T(1,128)S(1)}, u32[]{:S(2)}, u32[]{:S(2)}) async-start(f32[1,128,32]{1,0,2:T(1,128)} %bitcast.98), calls=%async_computation.2 | async-start | bytes 32768 | tf_op jit(solution)/shard_map/all_to_all | solution.py:45
  17.5 37.7 %copy-start.3 = (bf16[1,128,2048]{2,1,0:T(8,128)(2,1)S(1)}, bf16[1,128,2048]{2,1,0:T(8,128)(2,1)}, u32[]{:S(2)}) copy-start(bf16[1,128,2048]{2,1,0:T(8,128)(2,1)} %param.5) | copy-start | bytes 1572868
  30.0 20.0 %all-to-all-start.1 = ((bf16[8,2,16384]{2,1,0:T(2,128)(2,1)}), bf16[8,2,16384]{2,1,0:T(2,128)(2,1)S(1)}, u32[]{:S(2)}, u32[]{:S(2)}) async-start(bf16[8,2,16384]{2,1,0:T(2,128)(2,1)} %reshape.70), calls=%async_computation.1 | async-start | bytes 1048576 | tf_op jit(solution)/shard_map/all_to_all | solution.py:42
  50.0 18.6 %all-to-all-start.3 = ((bf16[8,2,16384]{2,1,0:T(2,128)(2,1)}), bf16[8,2,16384]{2,1,0:T(2,128)(2,1)S(1)}, u32[]{:S(2)}, u32[]{:S(2)}) async-start(bf16[8,2,16384]{2,1,0:T(2,128)(2,1)} %reshape.66), calls=%async_computation.3 | async-start | bytes 1048576 | tf_op jit(solution)/shard_map/all_to_all | solution.py:43
  68.6 18.7 %all-to-all-start = ((bf16[8,2,16384]{2,1,0:T(2,128)(2,1)}), bf16[8,2,16384]{2,1,0:T(2,128)(2,1)S(1)}, u32[]{:S(2)}, u32[]{:S(2)}) async-start(bf16[8,2,16384]{2,1,0:T(2,128)(2,1)} %reshape.68), calls=%async_computation | async-start | bytes 1048576 | tf_op jit(solution)/shard_map/all_to_all | solution.py:41
  87.8 2.7 %copy-start = (bf16[1,4,128,256]{2,3,1,0:T(8,128)(2,1)S(1)}, bf16[1,4,128,256]{2,3,1,0:T(8,128)(2,1)}, u32[]{:S(2)}) copy-start(bf16[1,4,128,256]{2,3,1,0:T(8,128)(2,1)} %slice.45) | copy-start | bytes 786436
  87.8 3.1 %copy-start.1 = (bf16[1,4,128,256]{2,3,1,0:T(8,128)(2,1)S(1)}, bf16[1,4,128,256]{2,3,1,0:T(8,128)(2,1)}, u32[]{:S(2)}) copy-start(bf16[1,4,128,256]{2,3,1,0:T(8,128)(2,1)} %slice.43) | copy-start | bytes 786436
  93.6 1.5 %copy-start.4 = (bf16[1024,4,64]{0,2,1:T(8,128)(2,1)S(1)}, bf16[1024,4,64]{0,2,1:T(8,128)(2,1)}, u32[]{:S(2)}) copy-start(bf16[1024,4,64]{0,2,1:T(8,128)(2,1)} %reshape_squeeze.7) | copy-start | bytes 1572868
  93.6 1.5 %copy-start.5 = (bf16[512,4,64]{0,2,1:T(8,128)(2,1)S(1)}, bf16[512,4,64]{0,2,1:T(8,128)(2,1)}, u32[]{:S(2)}) copy-start(bf16[512,4,64]{0,2,1:T(8,128)(2,1)} %mul.15) | copy-start | bytes 786436
Sparse Core Ops, SparseCore 0:
  8.9 60.9 all-gather.1
where the time goes:
time: 139 us; the launch traced here: 138 us
  other arithmetic  43 us (31%)
  starting transfers between devices  24.4 us (18%)
  blocking collectives  17.2 us (12%)
  local copies, waits for them, and re-layouts  16.5 us (12%)
  between operations  13.7 us (10%)
  matrix products  13.1 us (9%)
  waiting for transfers between devices  10.5 us (8%)
    unnamed x4, other arithmetic  38.4 us
    all_to_all x1, blocking collectives, local(): lax.all_to_all(attended, 'sp', split_axis=1, concat_axis=2, tiled=True)  17.2 us
    unnamed x28, local copies, waits for them, and re-layouts  9.83 us
    all_to_all x1, waiting for transfers between devices, local(): lax.all_to_all(queries, 'sp', split_axis=2, concat_axis=1, tiled=True)  8.91 us
    all_to_all x1, starting transfers between devices, local(): lax.all_to_all(gate_totals, 'sp', split_axis=2, concat_axis=1, tiled=True)  7.29 us
    all_to_all x1, starting transfers between devices, local(): lax.all_to_all(keys, 'sp', split_axis=2, concat_axis=1, tiled=True)  6 us
    all_to_all x1, starting transfers between devices, local(): lax.all_to_all(queries, 'sp', split_axis=2, concat_axis=1, tiled=True)  5.88 us
    dot_general x1, matrix products, local(): jnp.dot(flat_rows, lax.all_gather(w_out, 'dp', axis=1, tiled=True), prefe...  5.46 us
  transfers between devices with their start and end apart: 5, of which 3 were waited for; matrix products, arithmetic and copies ran while one was open for 48% of the time, Pallas kernels for 0%

commit v1 on v0

v1 whole, which is shorter than its diff:
```python
import functools

import jax
import jax.numpy as jnp
from jax import lax
from jax.experimental import pallas as pl
from jax.experimental.pallas import tpu as pltpu
from jax.sharding import PartitionSpec as P

HEAD_DIM = 64
LANES = 128
W_CHUNKS = 8
MESH = pl.DeviceIdType.MESH


def attend(queries, key_rows, value_rows, totals):
    length = queries.shape[0]
    block_rows = min(length, 512)
    pieces = []
    for begin_row in range(0, length, block_rows):
        end_row = begin_row + block_rows
        scaled = queries[begin_row:end_row] * jnp.bfloat16(HEAD_DIM ** (-0.5))
        scores = jnp.einsum(
            "qhd,khd->hqk", scaled, key_rows[:end_row], preferred_element_type=jnp.float32
        )
        causal = jnp.arange(end_row)[None, :] <= (begin_row + jnp.arange(block_rows))[:, None]
        scores = jnp.where(
            causal[None],
            scores
            + jnp.transpose(totals[begin_row:end_row])[:, :, None]
            - jnp.transpose(totals[:end_row])[:, None, :],
            -jnp.inf,
        )
        biggest = jnp.max(scores, axis=-1, keepdims=True)
        expo = jnp.exp(scores - biggest)
        summed = jnp.sum(expo, axis=-1)
        weights = expo.astype(jnp.bfloat16)
        output = jnp.einsum(
            "hqk,khd->qhd", weights, value_rows[:end_row], preferred_element_type=jnp.float32
        )
        output = output / jnp.transpose(summed)[:, :, None]
        pieces.append(output.astype(jnp.bfloat16))
    return jnp.concatenate(pieces, axis=0).reshape(length, -1)


def general(queries, keys, values, gate_totals, w_out):
    moved = [
        lax.all_to_all(x, "sp", split_axis=2, concat_axis=1, tiled=True)
        for x in (queries, keys, values, gate_totals)
    ]
    length = moved[0].shape[1]
    heads = [x[0].reshape(length, -1, HEAD_DIM) for x in moved[:3]]
    attended = attend(heads[0], heads[1], heads[2], moved[3][0])[None]
    rows = lax.all_to_all(attended, "sp", split_axis=1, concat_axis=2, tiled=True)
    mixed = jnp.dot(
        rows[0],
        lax.all_gather(w_out, "dp", axis=1, tiled=True),
        preferred_element_type=jnp.float32,
    )
    return mixed.astype(jnp.bfloat16)[None]


def kernel(n, ndp, q_ref, k_ref, v_ref, g_ref, w_ref, o_ref,
           qb, kb, vb, gb, ob, att, wall, acc,
           in_send, in_recv, g_send, g_recv, own_sem, o_send, o_recv,
           y_send, y_recv, p_send, p_recv, f_send, f_recv):
    me = lax.axis_index("sp")
    me_dp = lax.axis_index("dp")
    core = lax.rem(me_dp, 2)
    row_y = lax.div(me_dp, 2)
    ny = ndp // 2
    partner = row_y * 2 + 1 - core
    L = q_ref.shape[0]
    length = n * L
    pairs = qb.shape[0]
    W = pairs * LANES
    w_rows, w_cols = w_ref.shape
    step_rows = w_rows // W_CHUNKS

    barrier = pltpu.get_barrier_semaphore()
    for d in range(1, n):
        pl.semaphore_signal(barrier, inc=1, device_id={"sp": lax.rem(me + d, n)}, device_id_type=MESH)
    pl.semaphore_signal(barrier, inc=1, device_id={"dp": partner}, device_id_type=MESH)
    for d in range(1, ny):
        pl.semaphore_signal(
            barrier, inc=1, device_id={"dp": lax.rem(row_y + d, ny) * 2 + core}, device_id_type=MESH
        )
    pl.semaphore_wait(barrier, n - 1 + 1 + ny - 1)

    def rows_of(rank):
        return pl.ds(pl.multiple_of(rank * L, L), L)

    def lanes_of(rank, c):
        return pl.ds(pl.multiple_of(rank * W + c * LANES, LANES), LANES)

    bufs = ((k_ref, kb), (q_ref, qb), (v_ref, vb))

    def in_copy(a, c, d):
        dest = lax.rem(me + d, n)
        src, dst = bufs[a]
        return pltpu.make_async_remote_copy(
            src_ref=src.at[:, lanes_of(dest, c)], dst_ref=dst.at[c, rows_of(me), :],
            send_sem=in_send.at[a, c, d], recv_sem=in_recv.at[a, c, d],
            device_id={"sp": dest}, device_id_type=MESH)

    def in_own(a, c):
        src, dst = bufs[a]
        return pltpu.make_async_copy(src.at[:, lanes_of(me, c)], dst.at[c, rows_of(me), :], in_recv.at[a, c, 0])

    def g_copy(d):
        dest = lax.rem(me + d, n)
        return pltpu.make_async_remote_copy(
            src_ref=g_ref.at[dest], dst_ref=gb.at[me], send_sem=g_send.at[d], recv_sem=g_recv.at[d],
            device_id={"sp": dest}, device_id_type=MESH)

    def chunk(j):
        return pl.ds(j * step_rows, step_rows)

    def y_copy(d, j):
        return pltpu.make_async_remote_copy(
            src_ref=w_ref.at[chunk(j)], dst_ref=wall.at[me_dp, chunk(j)],
            send_sem=y_send.at[d, j], recv_sem=y_recv.at[d, j],
            device_id={"dp": lax.rem(row_y + d, ny) * 2 + core}, device_id_type=MESH)

    def source(d):
        return lax.rem(row_y + ny - d, ny) * 2

    def forward(d, j):
        held = source(d) + core
        return pltpu.make_async_remote_copy(
            src_ref=wall.at[held, chunk(j)], dst_ref=wall.at[held, chunk(j)],
            send_sem=f_send.at[d, j], recv_sem=f_recv.at[d, j],
            device_id={"dp": partner}, device_id_type=MESH)

    p_copy = pltpu.make_async_remote_copy(
        src_ref=w_ref, dst_ref=wall.at[me_dp], send_sem=p_send, recv_sem=p_recv,
        device_id={"dp": partner}, device_id_type=MESH)
    w_own = pltpu.make_async_copy(w_ref, wall.at[me_dp], own_sem.at[0])
    g_own = pltpu.make_async_copy(g_ref.at[me], gb.at[me], own_sem.at[1])

    for d in range(1, n):
        g_copy(d).start()
    for c in range(pairs):
        for d in range(1, n):
            for a in range(3):
                in_copy(a, c, d).start()
        if c == 0:
            for j in range(W_CHUNKS):
                for d in range(1, ny):
                    y_copy(d, j).start()
    g_own.start()
    for c in range(pairs):
        for a in range(3):
            in_own(a, c).start()
    p_copy.start()
    w_own.start()

    passed = [0]

    def pass_on(upto):
        for j in range(passed[0], min(upto, W_CHUNKS)):
            for d in range(1, ny):
                y_copy(d, j).wait_recv()
                forward(d, j).start()
        passed[0] = max(passed[0], min(upto, W_CHUNKS))

    def o_copy(c, d):
        dest = lax.rem(me + d, n)
        return pltpu.make_async_remote_copy(
            src_ref=ob.at[c, rows_of(dest), :], dst_ref=att.at[:, lanes_of(me, c)],
            send_sem=o_send.at[c, d], recv_sem=o_recv.at[c, d],
            device_id={"sp": dest}, device_id_type=MESH)

    def o_own(c):
        return pltpu.make_async_copy(ob.at[c, rows_of(me), :], att.at[:, lanes_of(me, c)], o_recv.at[c, 0])

    tile = 2 * L if n % 2 == 0 else L
    for c in range(pairs):
        if c == 0:
            g_own.wait()
            for d in range(1, n):
                g_copy(d).wait_recv()
        for a in range(3):
            in_own(a, c).wait()
        for d in range(1, n):
            for a in range(3):
                in_copy(a, c, d).wait_recv()
        for i in range(length // tile):
            kept = (i + 1) * tile
            rows = pl.ds(i * tile, tile)
            scaled = qb[c, rows, :] * jnp.bfloat16(HEAD_DIM ** -0.5)
            key_lane = lax.broadcasted_iota(jnp.int32, (kept, LANES), 1)
            out_lane = lax.broadcasted_iota(jnp.int32, (tile, LANES), 1)
            causal = lax.broadcasted_iota(jnp.int32, (tile, tile), 1) <= lax.broadcasted_iota(
                jnp.int32, (tile, tile), 0)
            keys = kb[c, pl.ds(0, kept), :]
            values = vb[c, pl.ds(0, kept), :]
            outs = []
            for h in range(2):
                mine = (key_lane < HEAD_DIM) if h == 0 else (key_lane >= HEAD_DIM)
                head_keys = jnp.where(mine, keys, jnp.zeros_like(keys))
                scores = lax.dot_general(
                    scaled, head_keys, (((1,), (1,)), ((), ())), preferred_element_type=jnp.float32)
                gates = jnp.concatenate(
                    [gb[b, 2 * c + h:2 * c + h + 1, :] for b in range(kept // L)], axis=1)
                scores = scores - gates
                last = jnp.where(causal, scores[:, kept - tile:], -jnp.inf)
                scores = last if i == 0 else jnp.concatenate([scores[:, :kept - tile], last], axis=1)
                peak = jnp.max(scores, axis=1, keepdims=True)
                expo = jnp.exp(scores - peak)
                total = jnp.sum(expo, axis=1, keepdims=True)
                outs.append(jnp.dot(
                    expo.astype(jnp.bfloat16), values, preferred_element_type=jnp.float32) / total)
            ob[c, rows, :] = jnp.where(out_lane < HEAD_DIM, outs[0], outs[1]).astype(jnp.bfloat16)
        for d in range(1, n):
            o_copy(c, d).start()
        o_own(c).start()
        pass_on((c + 1) * W_CHUNKS // (pairs + 2))

    for c in range(pairs):
        o_own(c).wait()
        for d in range(1, n):
            o_copy(c, d).wait_recv()

    def columns(r):
        return pl.ds(pl.multiple_of(r * w_cols, LANES), w_cols)

    w_own.wait()
    o_ref[:, columns(me_dp)] = jnp.dot(
        att[...], wall[me_dp], preferred_element_type=jnp.float32).astype(o_ref.dtype)
    p_copy.wait_recv()
    o_ref[:, columns(partner)] = jnp.dot(
        att[...], wall[partner], preferred_element_type=jnp.float32).astype(o_ref.dtype)
    for j in range(W_CHUNKS):
        pass_on(j + 1)
        for d in range(1, ny):
            straight = source(d) + core
            crossed = source(d) + 1 - core
            left = att[:, j * step_rows:(j + 1) * step_rows]
            for which, r in ((0, straight), (1, crossed)):
                if which:
                    forward(d, j).wait_recv()
                part = jnp.dot(left, wall[r, chunk(j)], preferred_element_type=jnp.float32)
                if j > 0:
                    part = acc[d - 1, which] + part
                if j < W_CHUNKS - 1:
                    acc[d - 1, which] = part
                else:
                    o_ref[:, columns(r)] = part.astype(o_ref.dtype)

    p_copy.wait_send()
    for d in range(1, n):
        g_copy(d).wait_send()
        for c in range(pairs):
            o_copy(c, d).wait_send()
            for a in range(3):
                in_copy(a, c, d).wait_send()
    for j in range(W_CHUNKS):
        for d in range(1, ny):
            y_copy(d, j).wait_send()
            forward(d, j).wait_send()


def fused(n, ndp, queries, keys, values, gate_totals, w_out):
    L, model = queries.shape[1], queries.shape[2]
    heads = gate_totals.shape[2] // n
    pairs = heads * HEAD_DIM // LANES
    length = n * L
    ny = ndp // 2
    gates = jnp.transpose(gate_totals[0]).reshape(n, heads, L)
    w_rows, w_cols = w_out.shape
    bf16, f32 = jnp.bfloat16, jnp.float32
    dma = pltpu.SemaphoreType.DMA
    anywhere = pl.BlockSpec(memory_space=pl.ANY)
    out = pl.pallas_call(
        functools.partial(kernel, n, ndp),
        out_shape=jax.ShapeDtypeStruct((L, w_cols * ndp), bf16),
        in_specs=[anywhere] * 5,
        out_specs=pl.BlockSpec(memory_space=pltpu.VMEM),
        scratch_shapes=[
            pltpu.VMEM((pairs, length, LANES), bf16),
            pltpu.VMEM((pairs, length, LANES), bf16),
            pltpu.VMEM((pairs, length, LANES), bf16),
            pltpu.VMEM((n, heads, L), f32),
            pltpu.VMEM((pairs, length, LANES), bf16),
            pltpu.VMEM((L, model), bf16),
            pltpu.VMEM((ndp, w_rows, w_cols), bf16),
            pltpu.VMEM((max(ny - 1, 1), 2, L, w_cols), f32),
            dma((3, pairs, n)), dma((3, pairs, n)), dma((n,)), dma((n,)), dma((2,)),
            dma((pairs, n)), dma((pairs, n)),
            dma((ny, W_CHUNKS)), dma((ny, W_CHUNKS)), dma, dma,
            dma((ny, W_CHUNKS)), dma((ny, W_CHUNKS)),
        ],
        compiler_params=pltpu.CompilerParams(
            collective_id=0, has_side_effects=True, vmem_limit_bytes=48 * 1024 * 1024),
        name="fused_attention",
    )(queries[0], keys[0], values[0], gates, w_out)
    return out[None]


def solution(mesh):
    n, ndp = mesh.shape["sp"], mesh.shape["dp"]

    def local(queries, keys, values, gate_totals, w_out):
        width = queries.shape[2] // n
        fits = width % LANES == 0 and ndp % 2 == 0 and queries.shape[1] % LANES == 0
        if fits:
            return fused(n, ndp, queries, keys, values, gate_totals, w_out)
        return general(queries, keys, values, gate_totals, w_out)

    placed = (P("dp", "sp", None),) * 4 + (P(None, "dp"),)
    return jax.shard_map(
        local, mesh=mesh, in_specs=placed, out_specs=P("dp", "sp", None), check_vma=False)
```

time: 139 us -> 71.5 us (0.51)
  Pallas kernels: 0 us -> 64.9 us
  other arithmetic: 43 us -> 0 us
  starting transfers between devices: 24.4 us -> 0 us
  blocking collectives: 17.2 us -> 0 us
  between operations: 13.7 us -> 0.01 us
  matrix products: 13.1 us -> 0 us
  waiting for transfers between devices: 10.5 us -> 0 us
  local copies, waits for them, and re-layouts: 16.5 us -> 6.23 us
    pallas_call x0 -> x1, Pallas kernels: none -> 64.9 us  [fused(): pl.pallas_call(functools.partial(kernel, n, ndp), out_shape=jax.ShapeDtyp...]
    unnamed x4 -> x0, other arithmetic: 38.4 us -> none
    all_to_all x4 -> x0, starting transfers between devices: 24.4 us -> none  [the longest x1 7.29 us: local(): lax.all_to_all(gate_totals, 'sp', split_axis=2, concat_axis=1, tiled=True)]
    all_to_all x1 -> x0, blocking collectives: 17.2 us -> none  [local(): lax.all_to_all(attended, 'sp', split_axis=1, concat_axis=2, tiled=True)]
    dot_general x5 -> x0, matrix products: 13.1 us -> none  [the longest x1 5.46 us: local(): jnp.dot(flat_rows, lax.all_gather(w_out, 'dp', axis=1, tiled=True), prefe...]
    all_to_all x4 -> x0, waiting for transfers between devices: 9.79 us -> none  [the longest x1 8.91 us: local(): lax.all_to_all(queries, 'sp', split_axis=2, concat_axis=1, tiled=True)]
    reduce_sum x2 -> x0, other arithmetic: 4.05 us -> none  [attend(): summed = jnp.sum(expo, axis=-1)]
    unnamed x28 -> x11, local copies, waits for them, and re-layouts: 9.83 us -> 6.23 us
  transfers between devices with their start and end apart: 5 -> 0, of which waited for: 3 -> 0; matrix products, arithmetic and copies ran while one was open for 48% -> 0% of each run, Pallas kernels for 0% -> 0%
where the time goes in v1:
time: 71.5 us; the launch traced here: 71.2 us
  Pallas kernels  64.9 us (91%)
  local copies, waits for them, and re-layouts  6.23 us (9%)
    pallas_call x1, Pallas kernels, fused(): pl.pallas_call(functools.partial(kernel, n, ndp), out_shape=jax.ShapeDtyp...  64.9 us
    unnamed x11, local copies, waits for them, and re-layouts  6.23 us

profile of v1, /device:TPU:0, one launch (start us, length us, event | category | flops | bytes accessed | tf_op | source)
XLA Modules:
  0.0 71.2 jit_solution(7538104217080750716)
XLA Ops:
  0.0 0.0 copy-start
  0.0 1.6 %copy-done = bf16[2048,512]{1,0:T(8,128)(2,1)S(1)} copy-done((bf16[2048,512]{1,0:T(8,128)(2,1)S(1)}, bf16[2048,512]{1,0:T(8,128)(2,1)}, u32[]{:S(2)}) %copy-start) | copy-done | bytes 2097176
  1.6 0.0 copy-start.1
  1.6 1.0 %copy-done.1 = bf16[1,128,2048]{2,1,0:T(8,128)(2,1)S(1)} copy-done((bf16[1,128,2048]{2,1,0:T(8,128)(2,1)S(1)}, bf16[1,128,2048]{2,1,0:T(8,128)(2,1)}, u32[]{:S(2)}) %copy-start.1) | copy-done | bytes 524312
  2.6 0.0 copy-start.2
  2.6 1.0 %copy-done.2 = bf16[1,128,2048]{2,1,0:T(8,128)(2,1)S(1)} copy-done((bf16[1,128,2048]{2,1,0:T(8,128)(2,1)S(1)}, bf16[1,128,2048]{2,1,0:T(8,128)(2,1)}, u32[]{:S(2)}) %copy-start.2) | copy-done | bytes 524312
  3.7 0.0 copy-start.3
  3.7 1.0 %copy-done.3 = bf16[1,128,2048]{2,1,0:T(8,128)(2,1)S(1)} copy-done((bf16[1,128,2048]{2,1,0:T(8,128)(2,1)S(1)}, bf16[1,128,2048]{2,1,0:T(8,128)(2,1)}, u32[]{:S(2)}) %copy-start.3) | copy-done | bytes 524312
  4.7 0.0 copy-start.4
  4.7 0.7 %copy-done.4 = f32[1,128,32]{1,2,0:T(8,128)S(1)} copy-done((f32[1,128,32]{1,2,0:T(8,128)S(1)}, f32[1,128,32]{1,2,0:T(8,128)}, u32[]{:S(2)}) %copy-start.4) | copy-done | bytes 16408
  5.4 64.9 %fused_attention.1 = bf16[128,2048]{1,0:T(8,128)(2,1)S(1)} custom-call(bf16[128,2048]{1,0:T(8,128)(2,1)S(1)} %bitcast.10, bf16[128,2048]{1,0:T(8,128)(2,1)S(1)} %bitcast.11, bf16[128,2048]{1,0:T(8,128)(2,1)S(1)} %bitcast.12, f32[8,4,128]{2,1,0:T(4,128)S(1)} %bitcast.13, bf16[2048,512]{1,0:T(8,128)(2,1)S(1)} %copy-done), custom_call_target="tpu_custom_call" | custom-call | tf_op jit(solution)/shard_map/fused_attention/pallas_call | solution.py:275
  70.4 0.8 %copy.7 = bf16[1,128,2048]{2,1,0:T(8,128)(2,1)} copy(bf16[1,128,2048]{2,1,0:T(8,128)(2,1)S(1)} %bitcast.9) | data formatting | bytes 1048576
Async XLA Ops:
  0.0 1.6 %copy-start = (bf16[2048,512]{1,0:T(8,128)(2,1)S(1)}, bf16[2048,512]{1,0:T(8,128)(2,1)}, u32[]{:S(2)}) copy-start(bf16[2048,512]{1,0:T(8,128)(2,1)} %w_ref.1) | copy-start | bytes 6291460
  1.6 1.0 %copy-start.1 = (bf16[1,128,2048]{2,1,0:T(8,128)(2,1)S(1)}, bf16[1,128,2048]{2,1,0:T(8,128)(2,1)}, u32[]{:S(2)}) copy-start(bf16[1,128,2048]{2,1,0:T(8,128)(2,1)} %param.5) | copy-start | bytes 1572868
  2.6 1.0 %copy-start.2 = (bf16[1,128,2048]{2,1,0:T(8,128)(2,1)S(1)}, bf16[1,128,2048]{2,1,0:T(8,128)(2,1)}, u32[]{:S(2)}) copy-start(bf16[1,128,2048]{2,1,0:T(8,128)(2,1)} %param.6) | copy-start | bytes 1572868
  3.7 1.0 %copy-start.3 = (bf16[1,128,2048]{2,1,0:T(8,128)(2,1)S(1)}, bf16[1,128,2048]{2,1,0:T(8,128)(2,1)}, u32[]{:S(2)}) copy-start(bf16[1,128,2048]{2,1,0:T(8,128)(2,1)} %param.7) | copy-start | bytes 1572868
  4.7 0.7 %copy-start.4 = (f32[1,128,32]{1,2,0:T(8,128)S(1)}, f32[1,128,32]{1,2,0:T(8,128)}, u32[]{:S(2)}) copy-start(f32[1,128,32]{1,2,0:T(8,128)} %param.8) | copy-start | bytes 49156

commit v2 on v0

v2 whole, which is shorter than its diff:
```python
import functools

import jax
import jax.numpy as jnp
from jax import lax
from jax.experimental import pallas as pl
from jax.experimental.pallas import tpu as pltpu
from jax.sharding import PartitionSpec as P

HEAD_DIM = 64
LANES = 128
W_CHUNKS = 8
MESH = pl.DeviceIdType.MESH


def attend(queries, key_rows, value_rows, totals):
    length = queries.shape[0]
    block_rows = min(length, 512)
    pieces = []
    for begin_row in range(0, length, block_rows):
        end_row = begin_row + block_rows
        scaled = queries[begin_row:end_row] * jnp.bfloat16(HEAD_DIM ** (-0.5))
        scores = jnp.einsum(
            "qhd,khd->hqk", scaled, key_rows[:end_row], preferred_element_type=jnp.float32
        )
        causal = jnp.arange(end_row)[None, :] <= (begin_row + jnp.arange(block_rows))[:, None]
        scores = jnp.where(
            causal[None],
            scores
            + jnp.transpose(totals[begin_row:end_row])[:, :, None]
            - jnp.transpose(totals[:end_row])[:, None, :],
            -jnp.inf,
        )
        biggest = jnp.max(scores, axis=-1, keepdims=True)
        expo = jnp.exp(scores - biggest)
        summed = jnp.sum(expo, axis=-1)
        weights = expo.astype(jnp.bfloat16)
        output = jnp.einsum(
            "hqk,khd->qhd", weights, value_rows[:end_row], preferred_element_type=jnp.float32
        )
        output = output / jnp.transpose(summed)[:, :, None]
        pieces.append(output.astype(jnp.bfloat16))
    return jnp.concatenate(pieces, axis=0).reshape(length, -1)


def general(queries, keys, values, gate_totals, w_out):
    moved = [
        lax.all_to_all(x, "sp", split_axis=2, concat_axis=1, tiled=True)
        for x in (queries, keys, values, gate_totals)
    ]
    length = moved[0].shape[1]
    heads = [x[0].reshape(length, -1, HEAD_DIM) for x in moved[:3]]
    attended = attend(heads[0], heads[1], heads[2], moved[3][0])[None]
    rows = lax.all_to_all(attended, "sp", split_axis=1, concat_axis=2, tiled=True)
    mixed = jnp.dot(
        rows[0],
        lax.all_gather(w_out, "dp", axis=1, tiled=True),
        preferred_element_type=jnp.float32,
    )
    return mixed.astype(jnp.bfloat16)[None]


def attend_rows(queries, parts, diagonal):
    rows = queries.shape[0]
    scaled = queries * jnp.bfloat16(HEAD_DIM ** -0.5)
    lane = lax.broadcasted_iota(jnp.int32, (rows, LANES), 1)
    outs, sums = [], []
    for h in range(2):
        mine = (lane < HEAD_DIM) if h == 0 else (lane >= HEAD_DIM)
        scores = []
        for at, (keys, _, gates) in enumerate(parts):
            head_keys = jnp.where(mine, keys, jnp.zeros_like(keys))
            score = lax.dot_general(
                scaled, head_keys, (((1,), (1,)), ((), ())), preferred_element_type=jnp.float32)
            score = score - gates[h:h + 1, :]
            if diagonal and at == len(parts) - 1:
                causal = lax.broadcasted_iota(jnp.int32, score.shape, 1) <= lax.broadcasted_iota(
                    jnp.int32, score.shape, 0)
                score = jnp.where(causal, score, -jnp.inf)
            scores.append(score)
        peak = functools.reduce(jnp.maximum, [jnp.max(x, axis=1, keepdims=True) for x in scores])
        expo = [jnp.exp(x - peak) for x in scores]
        total = sum(jnp.sum(x, axis=1, keepdims=True) for x in expo)
        out = sum(
            jnp.dot(x.astype(jnp.bfloat16), part[1], preferred_element_type=jnp.float32)
            for x, part in zip(expo, parts))
        outs.append(out / total)
        sums.append(peak + jnp.log(total))
    first = lane < HEAD_DIM
    return jnp.where(first, outs[0], outs[1]), jnp.where(first, sums[0], sums[1])


def kernel(n, ndp, q_ref, k_ref, v_ref, g_ref, w_ref, o_ref,
           qx, kx, vx, kz, vz, qz, gb, ob, held_o, held_l, part_o, part_l, got_o, got_l, att, wall, acc,
           x_send, x_recv, g_send, g_recv, own_sem, z_send, z_recv, po_send, po_recv, pl_send, pl_recv,
           o_send, o_recv, y_send, y_recv, wx_send, wx_recv, p_send, p_recv, f_send, f_recv):
    me = lax.axis_index("sp")
    x = lax.rem(me, 2)
    z = lax.div(me, 2)
    side = me + 1 - 2 * x
    me_dp = lax.axis_index("dp")
    core = lax.rem(me_dp, 2)
    row_y = lax.div(me_dp, 2)
    across = (1 - row_y) * 2 + core
    partner = row_y * 2 + 1 - core
    L = q_ref.shape[0]
    pairs = qx.shape[0]
    W = pairs * LANES
    w_rows, w_cols = w_ref.shape
    step_rows = w_rows // W_CHUNKS
    lent = W_CHUNKS // 4
    direct = W_CHUNKS - lent

    barrier = pltpu.get_barrier_semaphore()
    for d in range(1, n):
        pl.semaphore_signal(barrier, inc=1, device_id={"sp": lax.rem(me + d, n)}, device_id_type=MESH)
    for other in (partner, across):
        pl.semaphore_signal(barrier, inc=1, device_id={"dp": other}, device_id_type=MESH)
    pl.semaphore_wait(barrier, n + 1)

    def remote(src, dst, send, recv, **device):
        return pltpu.make_async_remote_copy(
            src_ref=src, dst_ref=dst, send_sem=send, recv_sem=recv, device_id=device, device_id_type=MESH)

    def rows_of(which):
        return pl.ds(pl.multiple_of(which * L, L), L)

    def lanes_of(which, p):
        return pl.ds(pl.multiple_of(which * W + p * LANES, LANES), LANES)

    bufs = ((q_ref, qx), (k_ref, kx), (v_ref, vx))

    def x_copy(a, p):
        src, dst = bufs[a]
        return remote(src.at[:, lanes_of(1 - x, p)], dst.at[p, rows_of(x), :],
                      x_send.at[a, p], x_recv.at[a, p], sp=side)

    def x_own(a, p):
        src, dst = bufs[a]
        return pltpu.make_async_copy(src.at[:, lanes_of(x, p)], dst.at[p, rows_of(x), :], own_sem.at[a, p])

    def g_copy(d):
        dest = lax.rem(me + d, n)
        return remote(g_ref.at[lax.rem(dest, 2)], gb.at[me], g_send.at[d], g_recv.at[d], sp=dest)

    g_own = pltpu.make_async_copy(g_ref.at[x], gb.at[me], g_recv.at[0])

    def chunk(s):
        if s < lent:
            at = s + direct * x
        elif s < direct:
            at = s
        else:
            at = (s - direct) + direct * (1 - x)
        return pl.ds(pl.multiple_of(at * step_rows, step_rows), step_rows)

    def y_copy(s):
        return remote(w_ref.at[chunk(s)], wall.at[me_dp, chunk(s)], y_send.at[s], y_recv.at[s], dp=across)

    def lend(s):
        return remote(wall.at[across, chunk(s)], wall.at[across, chunk(s)], wx_send.at[s], wx_recv.at[s], sp=side)

    def forward(s):
        return remote(wall.at[across, chunk(s)], wall.at[across, chunk(s)], f_send.at[s], f_recv.at[s], dp=partner)

    p_copy = remote(w_ref, wall.at[me_dp], p_send, p_recv, dp=partner)
    w_own = pltpu.make_async_copy(w_ref, wall.at[me_dp], own_sem.at[3, 0])

    for p in range(pairs):
        for a in range(3):
            x_copy(a, p).start()
        if p == 0:
            for d in range(1, n):
                g_copy(d).start()
            for s in range(direct):
                y_copy(s).start()
            g_own.start()
        for a in range(3):
            x_own(a, p).start()
    p_copy.start()
    w_own.start()

    def pass_on(begin, end):
        for s in range(begin, end):
            if s < direct:
                y_copy(s).wait_recv()
            else:
                lend(s - direct).wait_recv()
            forward(s).start()
            if s < lent:
                lend(s).start()

    def arrived(p):
        for a in range(3):
            x_own(a, p).wait()
            x_copy(a, p).wait_recv()

    def to_z(src, dst, k, slot, p, target):
        return remote(src, dst, z_send.at[k, p], z_recv.at[slot, p], sp=target * 2 + x)

    def part_copies(k, slot, p, target):
        return (
            remote(part_o.at[k, p], got_o.at[slot, p], po_send.at[k, p], po_recv.at[slot, p], sp=target * 2 + x),
            remote(part_l.at[k, p], got_l.at[slot, p], pl_send.at[k, p], pl_recv.at[slot, p], sp=target * 2 + x),
        )

    def o_copy(p):
        return remote(ob.at[p, rows_of(1 - x), :], att.at[:, lanes_of(x, p)], o_send.at[p], o_recv.at[p], sp=side)

    def o_own(p):
        return pltpu.make_async_copy(ob.at[p, rows_of(x), :], att.at[:, lanes_of(x, p)], own_sem.at[3, 1 + p])

    def gates_of(block, p):
        return jnp.concatenate([gb[2 * block, p], gb[2 * block + 1, p]], axis=1)

    def finish(p, value):
        ob[p] = value.astype(jnp.bfloat16)
        o_copy(p).start()
        o_own(p).start()

    def share(p, k, slot, target, value, lse):
        part_o[k, p] = value.astype(jnp.bfloat16)
        turned = jnp.transpose(lse)
        part_l[k, p] = jnp.concatenate([turned[0:1], turned[HEAD_DIM:HEAD_DIM + 1]], axis=0)
        for copy in part_copies(k, slot, p, target):
            copy.start()

    def join(p, slots):
        outs, sums = [held_o[p]], [held_l[p]]
        for slot in slots:
            for copy in part_copies(0, slot, p, 0):
                copy.wait_recv()
            outs.append(got_o[slot, p].astype(jnp.float32))
            lse = got_l[slot, p]
            sums.append(jnp.transpose(jnp.concatenate(
                [jnp.broadcast_to(lse[h:h + 1], (HEAD_DIM, 2 * L)) for h in range(2)], axis=0)))
        peak = functools.reduce(jnp.maximum, sums)
        scale = [jnp.exp(s - peak) for s in sums]
        finish(p, sum(o * s for o, s in zip(outs, scale)) / sum(scale))

    def each(body, begin=0, end=None):
        def step(p, carry):
            body(p)
            return carry
        lax.fori_loop(begin, pairs if end is None else end, step, 0)

    def gates_here():
        g_own.wait()
        for d in range(1, n):
            g_copy(d).wait_recv()

    half = pairs // 2

    @pl.when(z == 0)
    def _():
        def push(p):
            arrived(p)
            to_z(kx.at[p], kz.at[p], 0, 0, p, 1).start()
            to_z(vx.at[p], vz.at[p], 1, 1, p, 1).start()
        each(push)
        gates_here()
        def work(p):
            finish(p, attend_rows(qx[p], [(kx[p], vx[p], gates_of(0, p))], True)[0])
        each(work)
        pass_on(0, lent)
        def left(p):
            to_z(kx.at[p], kz.at[p], 0, 0, p, 1).wait_send()
            to_z(vx.at[p], vz.at[p], 1, 1, p, 1).wait_send()
        each(left)

    @pl.when(z == 1)
    def _():
        gates_here()
        def work(p):
            arrived(p)
            to_z(kx.at[p], kz.at[p], 0, 0, p, 0).wait_recv()
            to_z(vx.at[p], vz.at[p], 1, 1, p, 0).wait_recv()
            lower = (kz[p], vz[p], gates_of(0, p))
            own = (kx[p], vx[p], gates_of(1, p))
            finish(p, attend_rows(qx[p], [lower, own], True)[0])
            for k in range(2):
                to_z(qx.at[p], qz.at[k, p], 0, 2 + k, p, 0).wait_recv()
                share(p, k, 0, 2 + k, *attend_rows(qz[k, p], [lower, own], False))
        each(work, 0, half)
        pass_on(0, lent)
        each(work, half)
        def left(p):
            for k in range(2):
                for copy in part_copies(k, 0, p, 2 + k):
                    copy.wait_send()
        each(left)

    @pl.when(z == 2)
    def _():
        def push(p):
            arrived(p)
            to_z(qx.at[p], qz.at[0, p], 0, 2, p, 1).start()
        each(push)
        gates_here()
        def work(p):
            own = (kx[p], vx[p], gates_of(2, p))
            held_o[p], held_l[p] = attend_rows(qx[p], [own], True)
            to_z(qx.at[p], qz.at[0, p], 0, 2, p, 1).wait_recv()
            share(p, 1, 1, 3, *attend_rows(qz[0, p], [own], False))
        each(work)
        pass_on(0, lent)
        each(lambda p: join(p, (0,)))
        def left(p):
            to_z(qx.at[p], qz.at[0, p], 0, 2, p, 1).wait_send()
            for copy in part_copies(1, 1, p, 3):
                copy.wait_send()
        each(left)

    @pl.when(z == 3)
    def _():
        def push(p):
            arrived(p)
            to_z(qx.at[p], qz.at[1, p], 0, 3, p, 1).start()
            to_z(qx.at[p], qz.at[0, p], 1, 2, p, 2).start()
        each(push)
        gates_here()
        def work(p):
            held_o[p], held_l[p] = attend_rows(qx[p], [(kx[p], vx[p], gates_of(3, p))], True)
        each(work)
        pass_on(0, lent)
        each(lambda p: join(p, (0, 1)))
        def left(p):
            to_z(qx.at[p], qz.at[1, p], 0, 3, p, 1).wait_send()
            to_z(qx.at[p], qz.at[0, p], 1, 2, p, 2).wait_send()
        each(left)

    def whole(p):
        o_own(p).wait()
        o_copy(p).wait_recv()
    each(whole)

    def columns(r):
        return pl.ds(pl.multiple_of(r * w_cols, LANES), w_cols)

    pass_on(lent, W_CHUNKS // 2)
    w_own.wait()
    o_ref[:, columns(me_dp)] = jnp.dot(
        att[...], wall[me_dp], preferred_element_type=jnp.float32).astype(o_ref.dtype)
    p_copy.wait_recv()
    o_ref[:, columns(partner)] = jnp.dot(
        att[...], wall[partner], preferred_element_type=jnp.float32).astype(o_ref.dtype)
    crossed = (1 - row_y) * 2 + 1 - core
    order = list(range(lent)) + list(range(direct, W_CHUNKS)) + list(range(lent, direct))
    for at, s in enumerate(order):
        if s >= W_CHUNKS // 2:
            pass_on(s, s + 1)
        left = att[:, chunk(s)]
        for which, r in ((0, across), (1, crossed)):
            if which:
                forward(s).wait_recv()
            part = jnp.dot(left, wall[r, chunk(s)], preferred_element_type=jnp.float32)
            if at > 0:
                part = acc[which] + part
            if at < W_CHUNKS - 1:
                acc[which] = part
            else:
                o_ref[:, columns(r)] = part.astype(o_ref.dtype)

    p_copy.wait_send()
    for d in range(1, n):
        g_copy(d).wait_send()
    def sent(p):
        o_copy(p).wait_send()
        for a in range(3):
            x_copy(a, p).wait_send()
    each(sent)
    for s in range(W_CHUNKS):
        if s < direct:
            y_copy(s).wait_send()
        if s < lent:
            lend(s).wait_send()
        forward(s).wait_send()


def fused(n, ndp, queries, keys, values, gate_totals, w_out):
    L, model = queries.shape[1], queries.shape[2]
    heads = gate_totals.shape[2] // 2
    pairs = heads * HEAD_DIM // LANES
    gates = jnp.transpose(gate_totals[0]).reshape(2, pairs, 2, L)
    w_rows, w_cols = w_out.shape
    bf16, f32 = jnp.bfloat16, jnp.float32
    dma = pltpu.SemaphoreType.DMA
    block = (pairs, 2 * L, LANES)
    out = pl.pallas_call(
        functools.partial(kernel, n, ndp),
        out_shape=jax.ShapeDtypeStruct((L, w_cols * ndp), bf16),
        in_specs=[pl.BlockSpec(memory_space=pl.ANY)] * 5,
        out_specs=pl.BlockSpec(memory_space=pltpu.VMEM),
        scratch_shapes=[
            *[pltpu.VMEM(block, bf16)] * 5,
            pltpu.VMEM((2,) + block, bf16),
            pltpu.VMEM((n, pairs, 2, L), f32),
            pltpu.VMEM(block, bf16),
            pltpu.VMEM(block, f32),
            pltpu.VMEM(block, f32),
            pltpu.VMEM((2,) + block, bf16),
            pltpu.VMEM((2, pairs, 2, 2 * L), f32),
            pltpu.VMEM((2,) + block, bf16),
            pltpu.VMEM((2, pairs, 2, 2 * L), f32),
            pltpu.VMEM((L, model), bf16),
            pltpu.VMEM((ndp, w_rows, w_cols), bf16),
            pltpu.VMEM((2, L, w_cols), f32),
            dma((3, pairs)), dma((3, pairs)), dma((n,)), dma((n,)), dma((4, pairs + 1)),
            dma((2, pairs)), dma((4, pairs)),
            dma((2, pairs)), dma((2, pairs)), dma((2, pairs)), dma((2, pairs)),
            dma((pairs,)), dma((pairs,)),
            dma((W_CHUNKS,)), dma((W_CHUNKS,)), dma((W_CHUNKS,)), dma((W_CHUNKS,)), dma, dma,
            dma((W_CHUNKS,)), dma((W_CHUNKS,)),
        ],
        compiler_params=pltpu.CompilerParams(
            collective_id=0, has_side_effects=True, vmem_limit_bytes=67043328),
        name="fused_attention",
    )(queries[0], keys[0], values[0], gates, w_out)
    return out[None]


def solution(mesh):
    n, ndp = mesh.shape["sp"], mesh.shape["dp"]

    def local(queries, keys, values, gate_totals, w_out):
        fits = n == 8 and ndp == 4 and queries.shape[1] % LANES == 0
        if fits:
            return fused(n, ndp, queries, keys, values, gate_totals, w_out)
        return general(queries, keys, values, gate_totals, w_out)

    placed = (P("dp", "sp", None),) * 4 + (P(None, "dp"),)
    return jax.shard_map(
        local, mesh=mesh, in_specs=placed, out_specs=P("dp", "sp", None), check_vma=False)
```

time: 139 us -> 61.7 us (0.44)
  the two profiles are of different devices: /device:TPU:0 before, /device:TPU:21 now
where the time goes in v2:
time: 61.7 us; the launch traced here: 61.5 us
  Pallas kernels  59.6 us (97%)
  local copies, waits for them, and re-layouts  1.88 us (3%)
    pallas_call x1, Pallas kernels, fused(): pl.pallas_call(functools.partial(kernel, n, ndp), out_shape=jax.ShapeDtyp...  59.6 us
    unnamed x1, local copies, waits for them, and re-layouts  1.88 us

profile of v2, /device:TPU:21, one launch (start us, length us, event | category | flops | bytes accessed | tf_op | source)
XLA Modules:
  0.0 61.5 jit_solution(17677655275298485599)
XLA Ops:
  0.0 59.6 %fused_attention.1 = bf16[128,2048]{1,0:T(8,128)(2,1)} custom-call(bf16[128,2048]{1,0:T(8,128)(2,1)} %bitcast.10, bf16[128,2048]{1,0:T(8,128)(2,1)} %bitcast.11, bf16[128,2048]{1,0:T(8,128)(2,1)} %bitcast.12, f32[2,8,2,128]{3,2,1,0:T(2,128)} %bitcast.13, bf16[2048,512]{1,0:T(8,128)(2,1)} %w_ref.1), custom_call_target="tpu_custom_call" | custom-call | tf_op jit(solution)/shard_map/fused_attention/pallas_call | solution.py:389
  59.6 1.9 %copy.7 = bf16[1,128,2048]{2,1,0:T(8,128)(2,1)} copy(bf16[1,128,2048]{2,1,0:T(8,128)(2,1)} %bitcast.9) | data formatting | bytes 1048576

commit v3 on v2

--- a/solution.py
+++ b/solution.py
@@ -112,11 +112,19 @@
     direct = W_CHUNKS - lent
 
     barrier = pltpu.get_barrier_semaphore()
-    for d in range(1, n):
-        pl.semaphore_signal(barrier, inc=1, device_id={"sp": lax.rem(me + d, n)}, device_id_type=MESH)
+    meets = {0: (1,), 1: (0, 2, 3), 2: (1, 3), 3: (1, 2)}
+    for here, others in meets.items():
+        @pl.when(z == here)
+        def _(others=others):
+            for other in others:
+                pl.semaphore_signal(barrier, inc=1, device_id={"sp": other * 2 + x}, device_id_type=MESH)
+    pl.semaphore_signal(barrier, inc=1, device_id={"sp": side}, device_id_type=MESH)
     for other in (partner, across):
         pl.semaphore_signal(barrier, inc=1, device_id={"dp": other}, device_id_type=MESH)
-    pl.semaphore_wait(barrier, n + 1)
+    for here, others in meets.items():
+        @pl.when(z == here)
+        def _(others=others):
+            pl.semaphore_wait(barrier, len(others) + 3)
 
     def remote(src, dst, send, recv, **device):
         return pltpu.make_async_remote_copy(
@@ -139,11 +147,8 @@
         src, dst = bufs[a]
         return pltpu.make_async_copy(src.at[:, lanes_of(x, p)], dst.at[p, rows_of(x), :], own_sem.at[a, p])
 
-    def g_copy(d):
-        dest = lax.rem(me + d, n)
-        return remote(g_ref.at[lax.rem(dest, 2)], gb.at[me], g_send.at[d], g_recv.at[d], sp=dest)
-
-    g_own = pltpu.make_async_copy(g_ref.at[x], gb.at[me], g_recv.at[0])
+    g_copy = remote(g_ref.at[1 - x], gb.at[me], g_send.at[0], g_recv.at[0], sp=side)
+    g_own = pltpu.make_async_copy(g_ref.at[x], gb.at[me], g_recv.at[1])
 
     def chunk(s):
         if s < lent:
@@ -170,8 +175,7 @@
         for a in range(3):
             x_copy(a, p).start()
         if p == 0:
-            for d in range(1, n):
-                g_copy(d).start()
+            g_copy.start()
             for s in range(direct):
                 y_copy(s).start()
             g_own.start()
@@ -246,19 +250,22 @@
 
     def gates_here():
         g_own.wait()
-        for d in range(1, n):
-            g_copy(d).wait_recv()
+        g_copy.wait_recv()
+
+    def gates_up(target):
+        return remote(gb.at[pl.ds(0, 2)], gb.at[pl.ds(0, 2)], g_send.at[1], g_recv.at[2], sp=target * 2 + x)
 
     half = pairs // 2
 
     @pl.when(z == 0)
     def _():
+        gates_here()
+        gates_up(1).start()
         def push(p):
             arrived(p)
             to_z(kx.at[p], kz.at[p], 0, 0, p, 1).start()
             to_z(vx.at[p], vz.at[p], 1, 1, p, 1).start()
         each(push)
-        gates_here()
         def work(p):
             finish(p, attend_rows(qx[p], [(kx[p], vx[p], gates_of(0, p))], True)[0])
         each(work)
@@ -267,10 +274,12 @@
             to_z(kx.at[p], kz.at[p], 0, 0, p, 1).wait_send()
             to_z(vx.at[p], vz.at[p], 1, 1, p, 1).wait_send()
         each(left)
+        gates_up(1).wait_send()
 
     @pl.when(z == 1)
     def _():
         gates_here()
+        gates_up(0).wait_recv()
         def work(p):
             arrived(p)
             to_z(kx.at[p], kz.at[p], 0, 0, p, 0).wait_recv()
@@ -329,6 +338,8 @@
             to_z(qx.at[p], qz.at[0, p], 1, 2, p, 2).wait_send()
         each(left)
 
+    pass_on(lent, W_CHUNKS)
+
     def whole(p):
         o_own(p).wait()
         o_copy(p).wait_recv()
@@ -337,7 +348,6 @@
     def columns(r):
         return pl.ds(pl.multiple_of(r * w_cols, LANES), w_cols)
 
-    pass_on(lent, W_CHUNKS // 2)
     w_own.wait()
     o_ref[:, columns(me_dp)] = jnp.dot(
         att[...], wall[me_dp], preferred_element_type=jnp.float32).astype(o_ref.dtype)
@@ -347,8 +357,6 @@
     crossed = (1 - row_y) * 2 + 1 - core
     order = list(range(lent)) + list(range(direct, W_CHUNKS)) + list(range(lent, direct))
     for at, s in enumerate(order):
-        if s >= W_CHUNKS // 2:
-            pass_on(s, s + 1)
         left = att[:, chunk(s)]
         for which, r in ((0, across), (1, crossed)):
             if which:
@@ -362,8 +370,7 @@
                 o_ref[:, columns(r)] = part.astype(o_ref.dtype)
 
     p_copy.wait_send()
-    for d in range(1, n):
-        g_copy(d).wait_send()
+    g_copy.wait_send()
     def sent(p):
         o_copy(p).wait_send()
         for a in range(3):
@@ -405,7 +412,7 @@
             pltpu.VMEM((L, model), bf16),
             pltpu.VMEM((ndp, w_rows, w_cols), bf16),
             pltpu.VMEM((2, L, w_cols), f32),
-            dma((3, pairs)), dma((3, pairs)), dma((n,)), dma((n,)), dma((4, pairs + 1)),
+            dma((3, pairs)), dma((3, pairs)), dma((2,)), dma((3,)), dma((4, pairs + 1)),
             dma((2, pairs)), dma((4, pairs)),
             dma((2, pairs)), dma((2, pairs)), dma((2, pairs)), dma((2, pairs)),
             dma((pairs,)), dma((pairs,)),

time: 61.7 us -> 55.2 us (0.89)
  the two profiles are of different devices: /device:TPU:21 before, /device:TPU:22 now
where the time goes in v3:
time: 55.2 us; the launch traced here: 55.1 us
  Pallas kernels  53.2 us (96%)
  local copies, waits for them, and re-layouts  1.88 us (3%)
    pallas_call x1, Pallas kernels, fused(): pl.pallas_call(functools.partial(kernel, n, ndp), out_shape=jax.ShapeDtyp...  53.2 us
    unnamed x1, local copies, waits for them, and re-layouts  1.88 us

profile of v3, /device:TPU:22, one launch (start us, length us, event | category | flops | bytes accessed | tf_op | source)
XLA Modules:
  0.0 55.1 jit_solution(17656053303320699971)
XLA Ops:
  0.0 53.2 %fused_attention.1 = bf16[128,2048]{1,0:T(8,128)(2,1)} custom-call(bf16[128,2048]{1,0:T(8,128)(2,1)} %bitcast.10, bf16[128,2048]{1,0:T(8,128)(2,1)} %bitcast.11, bf16[128,2048]{1,0:T(8,128)(2,1)} %bitcast.12, f32[2,8,2,128]{3,2,1,0:T(2,128)} %bitcast.13, bf16[2048,512]{1,0:T(8,128)(2,1)} %w_ref.1), custom_call_target="tpu_custom_call" | custom-call | tf_op jit(solution)/shard_map/fused_attention/pallas_call | solution.py:396
  53.2 1.9 %copy.7 = bf16[1,128,2048]{2,1,0:T(8,128)(2,1)} copy(bf16[1,128,2048]{2,1,0:T(8,128)(2,1)} %bitcast.9) | data formatting | bytes 1048576

commit v4 on v3

--- a/solution.py
+++ b/solution.py
@@ -9,7 +9,7 @@
 
 HEAD_DIM = 64
 LANES = 128
-W_CHUNKS = 8
+W_CHUNKS = 16
 MESH = pl.DeviceIdType.MESH
 
 
@@ -108,7 +108,7 @@
     W = pairs * LANES
     w_rows, w_cols = w_ref.shape
     step_rows = w_rows // W_CHUNKS
-    lent = W_CHUNKS // 4
+    lent = W_CHUNKS // 8
     direct = W_CHUNKS - lent
 
     barrier = pltpu.get_barrier_semaphore()

time: 55.2 us -> 53.1 us (0.962)
  the two profiles are of different devices: /device:TPU:22 before, /device:TPU:0 now
where the time goes in v4:
time: 53.1 us; the launch traced here: 52.7 us
  Pallas kernels  50.9 us (96%)
  local copies, waits for them, and re-layouts  1.88 us (4%)
    pallas_call x1, Pallas kernels, fused(): pl.pallas_call(functools.partial(kernel, n, ndp), out_shape=jax.ShapeDtyp...  50.9 us
    unnamed x1, local copies, waits for them, and re-layouts  1.88 us

profile of v4, /device:TPU:0, one launch (start us, length us, event | category | flops | bytes accessed | tf_op | source)
XLA Modules:
  0.0 52.7 jit_solution(12733717579833328101)
XLA Ops:
  0.0 50.9 %fused_attention.1 = bf16[128,2048]{1,0:T(8,128)(2,1)} custom-call(bf16[128,2048]{1,0:T(8,128)(2,1)} %bitcast.10, bf16[128,2048]{1,0:T(8,128)(2,1)} %bitcast.11, bf16[128,2048]{1,0:T(8,128)(2,1)} %bitcast.12, f32[2,8,2,128]{3,2,1,0:T(2,128)} %bitcast.13, bf16[2048,512]{1,0:T(8,128)(2,1)} %w_ref.1), custom_call_target="tpu_custom_call" | custom-call | tf_op jit(solution)/shard_map/fused_attention/pallas_call | solution.py:396
  50.9 1.9 %copy.7 = bf16[1,128,2048]{2,1,0:T(8,128)(2,1)} copy(bf16[1,128,2048]{2,1,0:T(8,128)(2,1)} %bitcast.9) | data formatting | bytes 1048576
